TPU v7x, 256 devices: a whole 4x4x8 slice. The times are simulated.
256 devices in a mesh: kv: 64 (over z, y, core), tp: 4 (over x).
Axes of the slice: x: 4, y: 4, z: 8, core: 2. Of those that a mesh axis runs over, the one named last changes fastest.
Arguments:
- x_piece: bfloat16 [1024, 2048], P('kv'), may hold values from -6 to 6
- x_decode: bfloat16 [64, 2048], P('kv'), may hold values from -6 to 6
- norm_gain: float32 [2048], replicated, may hold values from 0.1 to 1.9
- w_query: bfloat16 [2048, 1024], P(None, 'tp'), may hold values from -0.1875 to 0.1875
- w_key: bfloat16 [2048, 1024], P(None, 'tp'), may hold values from -0.1875 to 0.1875
- w_value: bfloat16 [2048, 1024], P(None, 'tp'), may hold values from -0.125 to 0.125
- w_out: bfloat16 [1024, 2048], P(None, 'tp'), may hold values from -0.1875 to 0.1875
- head_gain: float32 [128], replicated, may hold values from 0.1 to 1.9
- lambdas: float32 [8], P('tp'), may hold values from 0.3 to 0.8
- piece_keys: bfloat16 [32768, 8, 128], P('kv', 'tp'), may hold values from -300 to 300
- piece_values: bfloat16 [32768, 8, 128], P('kv', 'tp'), may hold values from -6 to 6
- cache_keys: bfloat16 [64, 2048, 8, 128], P('kv', None, 'tp'), may hold values from -300 to 300
- cache_values: bfloat16 [64, 2048, 8, 128], P('kv', None, 'tp'), may hold values from -6 to 6
- cache_lengths: int32 [64], P('kv'), may hold values from 1 to 2048, as said below
Outputs:
- piece_out: bfloat16 [1024, 2048], P('kv', 'tp')
- decode_out: bfloat16 [64, 2048], P('kv', 'tp')
Inputs may be any that keep to these rules, and one draw needn't show every extreme that they name: `cache_lengths`: some sequence has exactly 2048 filled slots.
All inputs are finite; a program needn't handle non-finite values.
Results may differ from a plain program's by a relative error of at most 0.013.
The roundings to bfloat16 on the way count: a program that leaves them out, or rounds other values in their place, can miss the bound.
Values may be sent and summed in bfloat16 or wider, within the bound.
A program may use at most 64 MiB of HBM per device.

v0:
```python
import math

import jax
import jax.numpy as jnp
from jax import lax
from jax.sharding import PartitionSpec as P

EPS = 1e-06


def sent_to_all(array, axis):
    length = lax.axis_size(axis)
    return lax.all_to_all(
        jnp.broadcast_to(array[None], (length, *array.shape)), axis, 0, 0, tiled=True
    )


def laid_out(blocks, dim):
    lengths = list(blocks.shape[1:])
    lengths[dim] *= blocks.shape[0]
    return jnp.moveaxis(blocks, 0, dim).reshape(lengths)


def gather_directly(array, axis, dim):
    blocks = sent_to_all(array, axis)
    return laid_out(blocks, dim)


def side_by_side(arrays, axis, split_dim, concat_dim, along):
    ends, at = ([], 0)
    for a in arrays[:-1]:
        at += a.shape[along]
        ends.append(at)
    both = jnp.concatenate(arrays, axis=along)
    return tuple(
        jnp.split(
            lax.all_to_all(both, axis, split_axis=split_dim, concat_axis=concat_dim, tiled=True),
            ends,
            axis=along,
        )
    )


def shards(
    x_piece,
    x_decode,
    norm_gain,
    w_query,
    w_key,
    w_value,
    w_out,
    head_gain,
    lambdas,
    piece_keys,
    piece_values,
    cache_keys,
    cache_values,
    cache_lengths,
):
    piece_rows = x_piece.shape[0]
    local_heads = lambdas.shape[0]
    pair_width = piece_keys.shape[2]
    half_width = pair_width // 2
    value_width = piece_values.shape[2]
    score_scale = 1.0 / math.sqrt(half_width)
    cached = piece_keys.shape[0]
    all_rows = jnp.concatenate([x_piece, x_decode], axis=0)
    row_count = all_rows.shape[0]
    rows32 = all_rows.astype(jnp.float32)
    normed = (
        rows32 * lax.rsqrt(jnp.mean(rows32 * rows32, axis=-1, keepdims=True) + EPS) * norm_gain
    ).astype(jnp.bfloat16)
    queries = (
        jnp.dot(normed, w_query, preferred_element_type=jnp.float32)
        .astype(jnp.bfloat16)
        .reshape(row_count, local_heads, pair_width)
    )
    new_keys = (
        jnp.dot(normed, w_key, preferred_element_type=jnp.float32)
        .astype(jnp.bfloat16)
        .reshape(row_count, local_heads, pair_width)
    )
    new_values = (
        jnp.dot(normed, w_value, preferred_element_type=jnp.float32)
        .astype(jnp.bfloat16)
        .reshape(row_count, local_heads, value_width)
    )
    keys_all = jnp.concatenate([piece_keys, new_keys[:piece_rows]], axis=0)
    values_all = jnp.concatenate([piece_values, new_values[:piece_rows]], axis=0)
    offset = lax.axis_index("kv") * piece_rows
    kv_count = lax.axis_size("kv")
    total_rows = piece_rows * kv_count
    key_index = jnp.arange(cached + piece_rows, dtype=jnp.int32)

    def block_terms(query_block, block_start):
        block_rows = query_block.shape[0]
        query_pos = block_start + jnp.arange(block_rows, dtype=jnp.int32)
        allowed = (key_index[None, :] < cached) | (
            key_index[None, :] - cached + offset <= query_pos[:, None]
        )
        results = []
        for which_map in range(2):
            lower = which_map * half_width
            scores = (
                jnp.einsum(
                    "qhd,khd->hqk",
                    query_block[:, :, lower : lower + half_width],
                    keys_all[:, :, lower : lower + half_width],
                    preferred_element_type=jnp.float32,
                )
                * score_scale
            )
            scores = jnp.where(allowed[None], scores, -jnp.inf)
            row_max = jnp.max(scores, axis=-1)
            weights = jnp.exp(scores - row_max[..., None])
            totals = jnp.sum(weights, axis=-1)
            mixed = jnp.einsum(
                "hqk,khd->qhd",
                weights.astype(jnp.bfloat16),
                values_all,
                preferred_element_type=jnp.float32,
            )
            results += [row_max, totals, mixed.reshape(block_rows, local_heads * value_width)]
        return tuple(results)

    stat_zeros = jnp.zeros((local_heads, total_rows), jnp.float32)
    value_zeros = jnp.zeros((total_rows, local_heads * value_width), jnp.float32)
    initial = (stat_zeros, stat_zeros, value_zeros, stat_zeros, stat_zeros, value_zeros)
    piece = gather_directly(queries[:piece_rows], "kv", 0)
    start = jnp.int32(0)
    block_rows = piece.shape[0]
    nblocks = block_rows // 512
    blocks = piece.reshape(nblocks, 512, local_heads, pair_width)
    starts = 512 * jnp.arange(nblocks, dtype=jnp.int32)
    mapped = lax.map(lambda inputs: block_terms(inputs[0], inputs[1]), (blocks, starts))
    results = []
    for index, entry in enumerate(mapped):
        if index % 3 == 2:
            results.append(entry.reshape(block_rows, local_heads * value_width))
        else:
            results.append(entry.transpose(1, 0, 2).reshape(local_heads, block_rows))
    results = tuple(results)
    updated = []
    for index in range(6):
        along = 0 if index % 3 == 2 else 1
        updated.append(
            lax.dynamic_update_slice_in_dim(initial[index], results[index], start, along)
        )
    partials = tuple(updated)
    moved_values = tuple(
        (
            part.astype(jnp.float32)
            for part in side_by_side(
                (partials[2].astype(jnp.bfloat16), partials[5].astype(jnp.bfloat16)), "kv", 0, 0, 1
            )
        )
    )
    moved_stats = side_by_side((partials[0], partials[1], partials[3], partials[4]), "kv", 1, 1, 0)
    own = []
    for which_map in range(2):
        maxima = moved_stats[2 * which_map].reshape(local_heads, kv_count, piece_rows)
        sums = moved_stats[2 * which_map + 1].reshape(local_heads, kv_count, piece_rows)
        weighted = moved_values[which_map].reshape(kv_count, piece_rows, local_heads * value_width)
        new_max = jnp.max(maxima, axis=1)
        factor = jnp.exp(maxima - new_max[:, None, :])
        value_factor = jnp.repeat(factor.transpose(1, 2, 0), value_width, axis=2)
        own += [new_max, jnp.sum(factor * sums, axis=1), jnp.sum(value_factor * weighted, axis=0)]
    lambda_wide = jnp.repeat(lambdas, value_width)[None, :]
    piece_mixed = own[2] / jnp.repeat(own[1].T, value_width, axis=1) - lambda_wide * own[
        5
    ] / jnp.repeat(own[4].T, value_width, axis=1)
    dec_query = queries[piece_rows:]
    own_keys = new_keys[piece_rows:]
    own_values = new_values[piece_rows:].astype(jnp.float32)
    slot_index = jnp.arange(cache_keys.shape[1], dtype=jnp.int32)
    slot_allowed = slot_index[None, None, :] < cache_lengths[:, None, None]
    dec_results = []
    for which_map in range(2):
        lower = which_map * half_width
        scores = (
            jnp.einsum(
                "bhd,bkhd->bhk",
                dec_query[:, :, lower : lower + half_width],
                cache_keys[:, :, :, lower : lower + half_width],
                preferred_element_type=jnp.float32,
            )
            * score_scale
        )
        scores = jnp.where(slot_allowed, scores, -jnp.inf)
        own_score = (
            jnp.einsum(
                "bhd,bhd->bh",
                dec_query[:, :, lower : lower + half_width],
                own_keys[:, :, lower : lower + half_width],
                preferred_element_type=jnp.float32,
            )
            * score_scale
        )
        row_max = jnp.maximum(jnp.max(scores, axis=-1), own_score)
        weights = jnp.exp(scores - row_max[..., None])
        own_weight = jnp.exp(own_score - row_max)
        totals = jnp.sum(weights, axis=-1) + own_weight
        mixed = jnp.einsum(
            "bhk,bkhd->bhd",
            weights.astype(jnp.bfloat16),
            cache_values,
            preferred_element_type=jnp.float32,
        )
        mixed = mixed + own_weight.astype(jnp.bfloat16).astype(jnp.float32)[..., None] * own_values
        dec_results.append(mixed / totals[..., None])
    dec_mixed = (dec_results[0] - lambdas[None, :, None] * dec_results[1]).reshape(
        -1, local_heads * value_width
    )
    attended = jnp.concatenate([piece_mixed, dec_mixed], axis=0).reshape(
        row_count, local_heads, value_width
    )
    head_out = (
        attended
        * lax.rsqrt(jnp.mean(attended * attended, axis=-1, keepdims=True) + EPS)
        * head_gain
    ).astype(jnp.bfloat16)
    head_out = head_out.reshape(row_count, local_heads * value_width)
    output = jnp.dot(gather_directly(head_out, "tp", 1), w_out, preferred_element_type=jnp.float32)
    output = output.astype(jnp.bfloat16)
    return (output[:piece_rows], output[piece_rows:])


def solution(mesh):
    placed = (
        P("kv", None),
        P("kv", None),
        P(),
        P(None, "tp"),
        P(None, "tp"),
        P(None, "tp"),
        P(None, "tp"),
        P(),
        P("tp"),
        P("kv", "tp", None),
        P("kv", "tp", None),
        P("kv", None, "tp", None),
        P("kv", None, "tp", None),
        P("kv"),
    )
    return jax.shard_map(
        shards,
        mesh=mesh,
        in_specs=placed,
        out_specs=(P("kv", "tp"), P("kv", "tp")),
        check_vma=False,
    )
```

profile of v0, /device:TPU:2, one launch (start us, length us, event | category | flops | bytes accessed | tf_op | source)
XLA Modules:
  0.0 145.8 jit_solution(14942968073056447797)
XLA Ops:
  1.9 1.6 %convolution_convert_fusion.3 = bf16[17,256]{1,0:T(8,128)(2,1)S(1)} fusion(bf16[2048,256]{1,0:T(8,128)(2,1)} %param.19, f32[2048]{0:T(1024)} %param.18, f32[17]{0:T(128)S(1)} %add_rsqrt_fusion.1, bf16[1,2048]{1,0:T(2,128)(2,1)} %param.17, bf16[16,2048]{1,0:T(8,128)(2,1)} %param.16), kind=kOutput, calls=%fused_computation.46 | convolution fusion | flops 18073856 | bytes 1135172 | tf_op jit(solution)/shard_map/dot_general | solution.py:74
  4.4 12.4 %all-to-all-start = ((bf16[64,16,2,128]{3,1,2,0:T(8,128)(2,1)}), bf16[64,16,2,128]{3,1,2,0:T(8,128)(2,1)}, u32[]{:S(2)}, u32[]{:S(2)}) async-start(bf16[64,16,2,128]{3,1,2,0:T(8,128)(2,1)} %broadcast_in_dim.128), calls=%async_computation | async-start | bytes 1048576 | tf_op jit(solution)/shard_map/all_to_all | solution.py:13
  18.5 2.7 %slice_bitcast_fusion = (bf16[2048,2,64]{2,1,0:T(2,128)(2,1)S(1)}, bf16[2048,2,64]{2,1,0:T(2,128)(2,1)}) fusion(bf16[1,2048,2,128]{3,2,1,0:T(2,128)(2,1)S(1)} %copy-done.2), kind=kLoop, calls=%fused_computation.52 | loop fusion | bytes 2097152 | tf_op jit(solution)/shard_map/reshape.52
  23.8 1.7 %copy.65 = bf16[512,2,128]{2,0,1:T(8,128)(2,1)} copy(bf16[512,2,128]{2,1,0:T(2,128)(2,1)} %param.26) | data formatting | bytes 524288 | tf_op args[10]
  25.5 1.6 %fusion.33 = f32[2,1,2048]{2,1,0:T(1,128)S(1)} fusion(bf16[2048,2,64]{2,1,0:T(2,128)(2,1)} %get-tuple-element.319, bf16[2,64,1]{1,0,2:T(2,128)(2,1)} %get-tuple-element.331), kind=kOutput, calls=%fused_computation.50 | convolution fusion | flops 524288 | bytes 540928 | tf_op jit(solution)/shard_map/bhd,bkhd->bhk/dot_general | solution.py:181
  27.1 1.7 %fusion.31 = f32[2,1,2048]{2,1,0:T(1,128)} fusion(bf16[2048,2,64]{2,1,0:T(2,128)(2,1)S(1)} %get-tuple-element.318, bf16[2,64,1]{1,0,2:T(2,128)(2,1)} %get-tuple-element.330), kind=kOutput, calls=%fused_computation.48 | convolution fusion | flops 524288 | bytes 540928 | tf_op jit(solution)/shard_map/bhd,bkhd->bhk/dot_general | solution.py:181
  28.8 1.4 fusion.66
  31.7 1.7 %pad_maximum_fusion.2 = bf16[528,2,128]{2,0,1:T(8,128)(2,1)} fusion(bf16[16,2,128]{2,0,1:T(8,128)(2,1)S(1)} %copy_bitcast_fusion, bf16[512,2,128]{2,0,1:T(8,128)(2,1)} %copy.65), kind=kLoop, calls=%fused_computation.63 | loop fusion | flops 540672 | bytes 540672 | tf_op jit(solution)/shard_map/concatenate | solution.py:89
  34.8 1.9 %copy.62 = bf16[64,16,2,128]{3,1,0,2:T(8,128)(2,1)} copy(bf16[64,16,2,128]{3,1,2,0:T(8,128)(2,1)} %all-to-all-done) | data formatting | bytes 1048576 | tf_op jit(solution)/shard_map/all_to_all | solution.py:13
  36.6 33.4 %while.24 = (s32[]{:T(128)}, f32[2,2,512]{2,1,0:T(2,128)}, f32[2,2,512]{2,1,0:T(2,128)}, bf16[2,512,256]{2,1,0:T(8,128)(2,1)}, f32[2,2,512]{2,1,0:T(2,128)}, /*i...) while((s32[]{:T(128)}, f32[2,2,512]{2,1,0:T(2,128)}, ...), condition=%wide.region_6.7_spmd.clone.clone, body=%wide.region_1.6_spmd.clone.clone.sunk | while | flops 427669568 | bytes 24839804 | solution.py:135
  36.6 1.2 dynamic_slice.22
  40.6 1.5 %fusion.97 = f32[2,512,528]{1,2,0:T(8,128)S(1)} fusion(bf16[528,2,128]{0,2,1:T(8,128)(2,1)} %get-tuple-element.467, bf16[512,2,128]{0,2,1:T(8,128)(2,1)} %bitcast.146), kind=kOutput, calls=%fused_computation.24.clone.1 | convolution fusion | flops 69206016 | bytes 2457600 | tf_op jit(solution)/shard_map/while/body/eval_jaxpr/qhd,khd->hqk/dot_general | solution.py:105
  44.0 1.5 %fusion.100 = bf16[2,512,128]{1,2,0:T(8,128)(2,1)} fusion(bf16[528,2,128]{2,0,1:T(8,128)(2,1)S(1)} %copy-done.8, f32[2,512,528]{1,2,0:T(8,128)S(1)} %get-tuple-element.420, f32[2,512]{1,0:T(2,128)S(1)} %get-tuple-element.421, pred[512,528]{0,1:T(8,128)(4,1)S(1)} %compare_or_fusion.2), kind=kOutput, calls=%fused_computation.11.clone.1 | convolution fusion | flops 140574720 | bytes 2969600 | tf_op jit(solution)/shard_map/while/body/eval_jaxpr/hqk,khd->qhd/dot_general | solution.py:117
  45.5 1.8 %copy.165 = bf16[1,512,256]{2,1,0:T(8,128)(2,1)} copy(bf16[1,512,256]{1,2,0:T(8,128)(2,1)} %bitcast.149) | data formatting | bytes 524288 | tf_op jit(solution)/shard_map/while/body/jit(dynamic_update_index_in_dim)/dynamic_update_slice | solution.py:135
  47.3 2.5 %fusion.101 = bf16[2,512,128]{1,2,0:T(8,128)(2,1)} fusion(bf16[528,2,128]{2,0,1:T(8,128)(2,1)} %get-tuple-element.468, f32[2,512,528]{1,2,0:T(8,128)S(1)} %fusion.97, f32[2,512]{1,0:T(2,128)S(1)} %get-tuple-element.422, pred[512,528]{0,1:T(8,128)(4,1)S(1)} %compare_or_fusion.2), kind=kOutput, calls=%fused_computation.12.clone.1 | convolution fusion | flops 140574720 | bytes 2969600 | tf_op jit(solution)/shard_map/while/body/eval_jaxpr/hqk,khd->qhd/dot_general | solution.py:117
  50.9 1.8 %constant_dynamic-update-slice_fusion.3 = (bf16[2,512,256]{2,1,0:T(8,128)(2,1)}, bf16[2,512,256]{2,1,0:T(8,128)(2,1)}) fusion(bf16[2,512,256]{2,1,0:T(8,128)(2,1)} %get-tuple-element.450, bf16[1,512,256]{2,1,0:T(8,128)(2,1)} %copy.165, s32[]{:T(128)S(6)} %copy.180, bf16[2,512,256]{2,1,0:T(8,128)(2,1)} %get-tuple-element.447, ...), kind=kLoop, calls=%fused_computation.35.clone.1 | loop fusion | bytes 1048580 | tf_op jit(solution)/shard_map/while/body/jit(dynamic_update_index_in_dim)/dynamic_update_slice | solution.py:135
  53.3 1.2 dynamic_slice.22
  57.2 1.5 %fusion.97 = f32[2,512,528]{1,2,0:T(8,128)S(1)} fusion(bf16[528,2,128]{0,2,1:T(8,128)(2,1)} %get-tuple-element.467, bf16[512,2,128]{0,2,1:T(8,128)(2,1)} %bitcast.146), kind=kOutput, calls=%fused_computation.24.clone.1 | convolution fusion | flops 69206016 | bytes 2457600 | tf_op jit(solution)/shard_map/while/body/eval_jaxpr/qhd,khd->hqk/dot_general | solution.py:105
  60.7 1.5 %fusion.100 = bf16[2,512,128]{1,2,0:T(8,128)(2,1)} fusion(bf16[528,2,128]{2,0,1:T(8,128)(2,1)S(1)} %copy-done.8, f32[2,512,528]{1,2,0:T(8,128)S(1)} %get-tuple-element.420, f32[2,512]{1,0:T(2,128)S(1)} %get-tuple-element.421, pred[512,528]{0,1:T(8,128)(4,1)S(1)} %compare_or_fusion.2), kind=kOutput, calls=%fused_computation.11.clone.1 | convolution fusion | flops 140574720 | bytes 2969600 | tf_op jit(solution)/shard_map/while/body/eval_jaxpr/hqk,khd->qhd/dot_general | solution.py:117
  62.2 1.8 %copy.165 = bf16[1,512,256]{2,1,0:T(8,128)(2,1)} copy(bf16[1,512,256]{1,2,0:T(8,128)(2,1)} %bitcast.149) | data formatting | bytes 524288 | tf_op jit(solution)/shard_map/while/body/jit(dynamic_update_index_in_dim)/dynamic_update_slice | solution.py:135
  64.0 2.5 %fusion.101 = bf16[2,512,128]{1,2,0:T(8,128)(2,1)} fusion(bf16[528,2,128]{2,0,1:T(8,128)(2,1)} %get-tuple-element.468, f32[2,512,528]{1,2,0:T(8,128)S(1)} %fusion.97, f32[2,512]{1,0:T(2,128)S(1)} %get-tuple-element.422, pred[512,528]{0,1:T(8,128)(4,1)S(1)} %compare_or_fusion.2), kind=kOutput, calls=%fused_computation.12.clone.1 | convolution fusion | flops 140574720 | bytes 2969600 | tf_op jit(solution)/shard_map/while/body/eval_jaxpr/hqk,khd->qhd/dot_general | solution.py:117
  67.6 1.8 %constant_dynamic-update-slice_fusion.3 = (bf16[2,512,256]{2,1,0:T(8,128)(2,1)}, bf16[2,512,256]{2,1,0:T(8,128)(2,1)}) fusion(bf16[2,512,256]{2,1,0:T(8,128)(2,1)} %get-tuple-element.450, bf16[1,512,256]{2,1,0:T(8,128)(2,1)} %copy.165, s32[]{:T(128)S(6)} %copy.180, bf16[2,512,256]{2,1,0:T(8,128)(2,1)} %get-tuple-element.447, ...), kind=kLoop, calls=%fused_computation.35.clone.1 | loop fusion | bytes 1048580 | tf_op jit(solution)/shard_map/while/body/jit(dynamic_update_index_in_dim)/dynamic_update_slice | solution.py:135
  74.2 10.4 %all-to-all-start.1 = ((f32[64,1,128]{2,1,0:T(1,128)}), f32[64,1,128]{2,1,0:T(1,128)S(1)}, u32[]{:S(2)}, u32[]{:S(2)}) async-start(f32[64,1,128]{2,1,0:T(1,128)} %reshape.373), calls=%async_computation.1 | async-start | bytes 65536 | tf_op jit(solution)/shard_map/all_to_all | solution.py:37
  84.5 2.3 %pad_maximum_fusion = bf16[64,16,512]{2,1,0:T(8,128)(2,1)} fusion(bf16[64,16,256]{2,1,0:T(8,128)(2,1)} %bitcast.155, bf16[64,16,256]{2,1,0:T(8,128)(2,1)} %bitcast.154), kind=kLoop, calls=%fused_computation.47 | loop fusion | flops 2097152 | bytes 2097152 | tf_op jit(solution)/shard_map/concatenate | solution.py:34
  86.8 7.3 %all-to-all-done.1 = f32[64,1,128]{2,1,0:T(1,128)S(1)} async-done(((f32[64,1,128]{2,1,0:T(1,128)}), f32[64,1,128]{2,1,0:T(1,128)S(1)}, u32[]{:S(2)}, u32[]{:S(2)}) %all-to-all-start.1) | async-done | bytes 32800 | tf_op jit(solution)/shard_map/all_to_all | solution.py:37
  94.2 4.8 %all-to-all-start.2 = ((bf16[64,16,512]{2,1,0:T(8,128)(2,1)}), bf16[64,16,512]{2,1,0:T(8,128)(2,1)S(1)}, u32[]{:S(2)}, u32[]{:S(2)}) async-start(bf16[64,16,512]{2,1,0:T(8,128)(2,1)} %pad_maximum_fusion), calls=%async_computation.2 | async-start | bytes 2097152 | tf_op jit(solution)/shard_map/all_to_all | solution.py:37
  102.3 1.3 copy.78
  103.5 1.3 copy.73
  105.0 22.7 %all-to-all-done.2 = bf16[64,16,512]{2,1,0:T(8,128)(2,1)S(1)} async-done(((bf16[64,16,512]{2,1,0:T(8,128)(2,1)}), bf16[64,16,512]{2,1,0:T(8,128)(2,1)S(1)}, u32[]{:S(2)}, u32[]{:S(2)}) %all-to-all-start.2) | async-done | bytes 1048608 | tf_op jit(solution)/shard_map/all_to_all | solution.py:37
  129.4 1.7 %reshape.353 = f32[64,16,2,128]{3,2,1,0:T(2,128)S(1)} reshape(f32[1024,256]{1,0:T(8,128)} %get-tuple-element.316) | data formatting | bytes 2097152 | tf_op jit(solution)/shard_map/reshape | solution.py:163
  131.1 3.9 %multiply_reduce_fusion = (f32[16,2,128]{2,1,0:T(2,128)S(1)}, f32[16,2,128]{2,1,0:T(2,128)S(1)}) fusion(f32[64,16,2,128]{3,2,1,0:T(2,128)S(1)} %reshape.355, f32[64,16,2]{2,1,0:T(8,128)} %copy.78, f32[64,16,2,128]{3,2,1,0:T(2,128)S(1)} %reshape.353, f32[64,16,2]{2,1,0:T(8,128)} %copy.73), kind=kLoop, calls=%fused_computation.54 | loop fusion | flops 1040384 | bytes 2146304 | tf_op jit(solution)/shard_map/reduce_sum | solution.py:167
  135.5 8.7 %all_to_all.25 = bf16[4,17,256]{2,1,0:T(8,128)(2,1)S(1)} all-to-all(bf16[4,17,256]{2,1,0:T(8,128)(2,1)S(1)} %broadcast_in_dim.136), channel_id=1, replica_groups=mesh['kv'=64,'tp'=4] {'tp'}, dimensions={0} | all-to-all | bytes 69632 | tf_op jit(solution)/shard_map/all_to_all | solution.py:13
  (173 shorter events, 31.8 us)
Async XLA Ops:
  0.6 99.4 %copy-start = (bf16[1,2048,2,128]{3,2,1,0:T(2,128)(2,1)S(1)}, bf16[1,2048,2,128]{3,2,1,0:T(2,128)(2,1)}, u32[]{:S(2)}) copy-start(bf16[1,2048,2,128]{3,2,1,0:T(2,128)(2,1)} %param.28) | copy-start | bytes 3145732
  0.6 16.2 %copy-start.10 = (bf16[1,2048]{1,0:T(2,128)(2,1)S(1)}, bf16[1,2048]{1,0:T(2,128)(2,1)}, u32[]{:S(2)}) copy-start(bf16[1,2048]{1,0:T(2,128)(2,1)} %param.17) | copy-start | bytes 12292
  0.7 16.2 %copy-start.4 = (bf16[16,2048]{1,0:T(8,128)(2,1)S(1)}, bf16[16,2048]{1,0:T(8,128)(2,1)}, u32[]{:S(2)}) copy-start(bf16[16,2048]{1,0:T(8,128)(2,1)} %param.16) | copy-start | bytes 196612
  0.7 16.2 %copy-start.11 = (f32[2048]{0:T(1024)S(1)}, f32[2048]{0:T(1024)}, u32[]{:S(2)}) copy-start(f32[2048]{0:T(1024)} %param.18) | copy-start | bytes 24580
  0.7 16.2 %copy-start.5 = (bf16[2048,256]{1,0:T(8,128)(2,1)S(1)}, bf16[2048,256]{1,0:T(8,128)(2,1)}, u32[]{:S(2)}) copy-start(bf16[2048,256]{1,0:T(8,128)(2,1)} %param.20) | copy-start | bytes 3145732
  0.7 17.8 %copy-start.2 = (bf16[1,2048,2,128]{3,2,1,0:T(2,128)(2,1)S(1)}, bf16[1,2048,2,128]{3,2,1,0:T(2,128)(2,1)}, u32[]{:S(2)}) copy-start(bf16[1,2048,2,128]{3,2,1,0:T(2,128)(2,1)} %param.27) | copy-start | bytes 3145732
  1.9 19.4 %copy-start.22 = (f32[17]{0:T(128)}, f32[17]{0:T(128)S(1)}, u32[]{:S(2)}) copy-start(f32[17]{0:T(128)S(1)} %add_rsqrt_fusion.1) | copy-start | bytes 208
  4.4 30.4 %all-to-all-start = ((bf16[64,16,2,128]{3,1,2,0:T(8,128)(2,1)}), bf16[64,16,2,128]{3,1,2,0:T(8,128)(2,1)}, u32[]{:S(2)}, u32[]{:S(2)}) async-start(bf16[64,16,2,128]{3,1,2,0:T(8,128)(2,1)} %broadcast_in_dim.128), calls=%async_computation | async-start | bytes 1048576 | tf_op jit(solution)/shard_map/all_to_all | solution.py:13
  21.2 9.5 %copy-start.6 = (bf16[2048,256]{1,0:T(8,128)(2,1)S(1)}, bf16[2048,256]{1,0:T(8,128)(2,1)}, u32[]{:S(2)}) copy-start(bf16[2048,256]{1,0:T(8,128)(2,1)} %param.21) | copy-start | bytes 3145732
  30.1 6.5 %copy-start.23 = (f32[2]{0:T(128)}, f32[2]{0:T(128)S(1)}, u32[]{:S(2)}) copy-start(f32[2]{0:T(128)S(1)} %get-tuple-element.279) | copy-start | bytes 28
  31.7 4.9 %copy-start.12 = (bf16[17,256]{1,0:T(8,128)(2,1)}, bf16[17,256]{1,0:T(8,128)(2,1)S(1)}, u32[]{:S(2)}) copy-start(bf16[17,256]{1,0:T(8,128)(2,1)S(1)} %convolution_convert_fusion.1) | copy-start | bytes 26116
  40.6 1.6 %copy-start.3 = (bf16[528,2,128]{0,2,1:T(8,128)(2,1)S(1)}, bf16[528,2,128]{0,2,1:T(8,128)(2,1)}, u32[]{:S(2)}) copy-start(bf16[528,2,128]{0,2,1:T(8,128)(2,1)} %get-tuple-element.467) | copy-start | bytes 811012 | tf_op jit(solution)/shard_map/while
  44.0 3.4 %copy-start.15 = (f32[2,2,512]{2,1,0:T(2,128)}, f32[2,2,512]{2,1,0:T(2,128)S(1)}, u32[]{:S(2)}) copy-start(f32[2,2,512]{2,1,0:T(2,128)S(1)} %get-tuple-element.458) | copy-start | bytes 24580 | tf_op jit(solution)/shard_map/while
  44.0 3.3 %copy-start.17 = (f32[2,2,512]{2,1,0:T(2,128)}, f32[2,2,512]{2,1,0:T(2,128)S(1)}, u32[]{:S(2)}) copy-start(f32[2,2,512]{2,1,0:T(2,128)S(1)} %get-tuple-element.459) | copy-start | bytes 24580 | tf_op jit(solution)/shard_map/while
  47.3 5.4 %copy-start.18 = (f32[2,2,512]{2,1,0:T(2,128)S(1)}, f32[2,2,512]{2,1,0:T(2,128)}, u32[]{:S(2)}) copy-start(f32[2,2,512]{2,1,0:T(2,128)} %get-tuple-element.448) | copy-start | bytes 24580 | tf_op jit(solution)/shard_map/while
  47.3 5.4 %copy-start.20 = (f32[2,2,512]{2,1,0:T(2,128)S(1)}, f32[2,2,512]{2,1,0:T(2,128)}, u32[]{:S(2)}) copy-start(f32[2,2,512]{2,1,0:T(2,128)} %get-tuple-element.449) | copy-start | bytes 24580 | tf_op jit(solution)/shard_map/while
  57.2 1.5 %copy-start.3 = (bf16[528,2,128]{0,2,1:T(8,128)(2,1)S(1)}, bf16[528,2,128]{0,2,1:T(8,128)(2,1)}, u32[]{:S(2)}) copy-start(bf16[528,2,128]{0,2,1:T(8,128)(2,1)} %get-tuple-element.467) | copy-start | bytes 811012 | tf_op jit(solution)/shard_map/while
  60.6 3.4 %copy-start.15 = (f32[2,2,512]{2,1,0:T(2,128)}, f32[2,2,512]{2,1,0:T(2,128)S(1)}, u32[]{:S(2)}) copy-start(f32[2,2,512]{2,1,0:T(2,128)S(1)} %get-tuple-element.458) | copy-start | bytes 24580 | tf_op jit(solution)/shard_map/while
  60.6 3.3 %copy-start.17 = (f32[2,2,512]{2,1,0:T(2,128)}, f32[2,2,512]{2,1,0:T(2,128)S(1)}, u32[]{:S(2)}) copy-start(f32[2,2,512]{2,1,0:T(2,128)S(1)} %get-tuple-element.459) | copy-start | bytes 24580 | tf_op jit(solution)/shard_map/while
  64.0 5.4 %copy-start.18 = (f32[2,2,512]{2,1,0:T(2,128)S(1)}, f32[2,2,512]{2,1,0:T(2,128)}, u32[]{:S(2)}) copy-start(f32[2,2,512]{2,1,0:T(2,128)} %get-tuple-element.448) | copy-start | bytes 24580 | tf_op jit(solution)/shard_map/while
  64.0 5.4 %copy-start.20 = (f32[2,2,512]{2,1,0:T(2,128)S(1)}, f32[2,2,512]{2,1,0:T(2,128)}, u32[]{:S(2)}) copy-start(f32[2,2,512]{2,1,0:T(2,128)} %get-tuple-element.449) | copy-start | bytes 24580 | tf_op jit(solution)/shard_map/while
  74.1 24.9 %copy-start.25 = (f32[2]{0:T(128)S(1)}, f32[2]{0:T(128)}, u32[]{:S(2)}) copy-start(f32[2]{0:T(128)} %get-tuple-element.280) | copy-start | bytes 28
  74.1 24.9 %copy-start.28 = (f32[2]{0:T(128)S(1)}, f32[2]{0:T(128)}, u32[]{:S(2)}) copy-start(f32[2]{0:T(128)} %get-tuple-element.282) | copy-start | bytes 28
  74.1 24.9 %copy-start.9 = (f32[2,1,2048]{2,1,0:T(1,128)S(1)}, f32[2,1,2048]{2,1,0:T(1,128)}, u32[]{:S(2)}) copy-start(f32[2,1,2048]{2,1,0:T(1,128)} %fusion.31) | copy-start | bytes 49156
  74.1 24.9 %copy-start.13 = (pred[2048]{0:T(1024)(128)(4,1)S(1)}, pred[2048]{0:T(1024)(128)(4,1)}, u32[]{:S(2)}) copy-start(pred[2048]{0:T(1024)(128)(4,1)} %iota_compare_fusion.1) | copy-start | bytes 6148
  74.1 25.2 %copy-start.29 = (f32[128]{0:T(128)S(1)}, f32[128]{0:T(128)}, u32[]{:S(2)}) copy-start(f32[128]{0:T(128)} %param.23) | copy-start | bytes 1540
  74.2 25.9 %copy-start.24 = (f32[2]{0:T(128)S(1)}, f32[2]{0:T(128)}, u32[]{:S(2)}) copy-start(f32[2]{0:T(128)} %copy-done.23) | copy-start | bytes 28
  74.2 25.8 %copy-start.27 = (f32[2]{0:T(128)S(1)}, f32[2]{0:T(128)}, u32[]{:S(2)}) copy-start(f32[2]{0:T(128)} %get-tuple-element.281) | copy-start | bytes 28
  74.2 20.0 %all-to-all-start.1 = ((f32[64,1,128]{2,1,0:T(1,128)}), f32[64,1,128]{2,1,0:T(1,128)S(1)}, u32[]{:S(2)}, u32[]{:S(2)}) async-start(f32[64,1,128]{2,1,0:T(1,128)} %reshape.373), calls=%async_computation.1 | async-start | bytes 65536 | tf_op jit(solution)/shard_map/all_to_all | solution.py:37
  86.8 13.7 %copy-start.26 = (f32[2]{0:T(128)S(1)}, f32[2]{0:T(128)}, u32[]{:S(2)}) copy-start(f32[2]{0:T(128)} %param.24) | copy-start | bytes 28
  94.2 33.5 %all-to-all-start.2 = ((bf16[64,16,512]{2,1,0:T(8,128)(2,1)}), bf16[64,16,512]{2,1,0:T(8,128)(2,1)S(1)}, u32[]{:S(2)}, u32[]{:S(2)}) async-start(bf16[64,16,512]{2,1,0:T(8,128)(2,1)} %pad_maximum_fusion), calls=%async_computation.2 | async-start | bytes 2097152 | tf_op jit(solution)/shard_map/all_to_all | solution.py:37
  131.1 13.2 %copy-start.7 = (bf16[1024,512]{1,0:T(8,128)(2,1)S(1)}, bf16[1024,512]{1,0:T(8,128)(2,1)}, u32[]{:S(2)}) copy-start(bf16[1024,512]{1,0:T(8,128)(2,1)} %param.22) | copy-start | bytes 3145732
  (12 other events, 11.4 us)
where the time goes:
time: 148 us; the launch traced here: 146 us
  local copies, waits for them, and re-layouts  37.1 us (25%)
  waiting for transfers between devices  30.1 us (20%)
  starting transfers between devices  27.6 us (19%)
  other arithmetic  20.6 us (14%)
  matrix products  19.6 us (13%)
  blocking collectives  8.7 us (6%)
  between operations  1.86 us (1%)
    all_to_all x2, waiting for transfers between devices, side_by_side(): lax.all_to_all(both, axis, split_axis=split_dim, concat_axis=concat_dim,...  30.1 us
    all_to_all x2, starting transfers between devices, side_by_side(): lax.all_to_all(both, axis, split_axis=split_dim, concat_axis=concat_dim,...  15.2 us
    all_to_all x1, starting transfers between devices, sent_to_all(): lax.all_to_all(jnp.broadcast_to(array[None], (length, *array.shape)), axi...  12.4 us
    dynamic_update_slice x10, local copies, waits for them, and re-layouts, shards(): lax.map(lambda inputs: block_terms(inputs[0], inputs[1]), (blocks, starts))  9.45 us
    all_to_all x1, blocking collectives, sent_to_all(): lax.all_to_all(jnp.broadcast_to(array[None], (length, *array.shape)), axi...  8.7 us
    dot_general x4, matrix products, block_terms(): jnp.einsum('hqk,khd->qhd', weights.astype(jnp.bfloat16), values_all, pref...  7.99 us
    dynamic_slice x6, local copies, waits for them, and re-layouts, shards(): lax.map(lambda inputs: block_terms(inputs[0], inputs[1]), (blocks, starts))  6.17 us
    dot_general x4, matrix products, block_terms(): jnp.einsum('qhd,khd->hqk', query_block[:, :, lower:lower + half_width], k...  4.66 us
  transfers between devices with their start and end apart: 3, of which 2 were waited for; matrix products, arithmetic and copies ran while one was open for 17% of the time, Pallas kernels for 0%

commit v1 on v0

v1 whole, which is shorter than its diff:
```python
import functools

import jax
import jax.numpy as jnp
from jax import lax
from jax.experimental import pallas as pl
from jax.experimental.pallas import tpu as pltpu
from jax.sharding import PartitionSpec as P

EPS = 1e-06
MESH = pl.DeviceIdType.MESH
NT = (((1,), (1,)), ((), ()))
LAG = 1


def kernel(
    Z, Y, X,
    x_hbm, xd_hbm, gain_hbm, wq_hbm, wk_hbm, wv_hbm, wo_hbm, hg_hbm, lam, pk_hbm, pv_hbm,
    ck_hbm, cv_hbm, length,
    out_p, out_d,
    x_v, xd_v, gain_v, hg_v, w_v, wo_v, kraw, vraw, kd, vd, ck_v, cv_v, tmp,
    nkv, nkv_in, qbuf, ysend, ysst, yrecv, yrst, zsend, zsst, zrecv, zrst, hbuf, dbuf,
    lsem, ps, pr, qzs, qzr, qys, qyr, yds, ydr, yss, ysr, zds, zdr, zss, zsr, hs, hr, ds, dr,
):
    kv = lax.axis_index("kv")
    tp = lax.axis_index("tp")
    core = lax.rem(kv, 2)
    chip = lax.div(kv, 2)
    y = lax.rem(chip, Y)
    z = lax.div(chip, Y)
    rows = x_v.shape[0]
    npos = kraw.shape[1] // 2
    pairs = Z // 2

    def dev(zz, yy):
        return ((zz * Y + yy) * 2 + core, tp)

    partner = (chip * 2 + 1 - core, tp)

    def xdev(xx):
        return (kv, xx)

    def mod(a, n):
        return lax.rem(a + n, n)

    barrier = pltpu.get_barrier_semaphore()
    for d in range(1, Z):
        pl.semaphore_signal(barrier, inc=1, device_id=dev(mod(z + d, Z), y), device_id_type=MESH)
    for d in range(1, Y):
        pl.semaphore_signal(barrier, inc=1, device_id=dev(z, mod(y + d, Y)), device_id_type=MESH)
    for d in range(1, X):
        pl.semaphore_signal(barrier, inc=1, device_id=xdev(mod(tp + d, X)), device_id_type=MESH)
    pl.semaphore_signal(barrier, inc=1, device_id=partner, device_id_type=MESH)

    local = []

    def fetch(src, dst):
        copy = pltpu.make_async_copy(src, dst, lsem.at[len(local)])
        copy.start()
        local.append(copy)
        return copy

    c_x = fetch(x_hbm, x_v)
    c_xd = fetch(xd_hbm, xd_v)
    c_gain = fetch(gain_hbm, gain_v)
    c_wq = fetch(wq_hbm, w_v.at[0])
    c_wk = fetch(wk_hbm, w_v.at[1])
    c_wv = fetch(wv_hbm, w_v.at[2])
    c_pk = fetch(pk_hbm, kraw.at[0])
    c_pv = fetch(pv_hbm, vraw.at[0])
    c_ck = fetch(ck_hbm, ck_v)
    c_cv = fetch(cv_hbm, cv_v)
    c_wo = fetch(wo_hbm, wo_v)
    c_hg = fetch(hg_hbm, hg_v)

    def remote(src, dst, ssem, rsem, device):
        return pltpu.make_async_remote_copy(
            src_ref=src, dst_ref=dst, send_sem=ssem, recv_sem=rsem,
            device_id=device, device_id_type=MESH,
        )

    c_x.wait()
    c_xd.wait()
    c_gain.wait()
    gain = gain_v[...]

    def norm(v):
        v = v.astype(jnp.float32)
        return v * lax.rsqrt(jnp.mean(v * v, axis=-1, keepdims=True) + EPS) * gain

    normed_p = norm(x_v[...]).astype(jnp.bfloat16)
    normed_d = jnp.broadcast_to(norm(xd_v[...]), (16, x_v.shape[1])).astype(jnp.bfloat16)
    normed = jnp.concatenate([normed_p, normed_d], axis=0)

    def project(which):
        return jnp.dot(normed, w_v[which], preferred_element_type=jnp.float32).astype(jnp.bfloat16)

    c_wq.wait()
    queries = project(0) * jnp.bfloat16(0.125)
    qbuf[z, y] = queries[:rows]

    pl.semaphore_wait(barrier, Z + Y + X - 2)

    def q_z(d):
        return remote(qbuf.at[z, y], qbuf.at[z, y], qzs.at[d], qzr.at[d], dev(mod(z + d, Z), y))

    def q_z_in(d):
        src = mod(z + Z - d, Z)
        return remote(qbuf.at[src, y], qbuf.at[src, y], qzs.at[d], qzr.at[d], dev(src, y))

    def q_y(o, e):
        zz = mod(z + o, Z)
        return remote(
            qbuf.at[zz, y], qbuf.at[zz, y], qys.at[o, e], qyr.at[o, e], dev(z, mod(y + e, Y))
        )

    def q_y_in(o, e):
        zz = mod(z + o, Z)
        src = mod(y + Y - e, Y)
        return remote(qbuf.at[zz, src], qbuf.at[zz, src], qys.at[o, e], qyr.at[o, e], dev(z, src))

    zorder = []
    for d in range(1, Z // 2 + 1):
        zorder.append(d)
        if Z - d not in zorder:
            zorder.append(Z - d)
    for d in reversed(zorder):
        q_z(d).start()
    for e in range(1, Y):
        q_y(0, e).start()

    p_k = remote(pk_hbm, kraw.at[1], ps.at[0], pr.at[0], partner)
    p_v = remote(pv_hbm, vraw.at[1], ps.at[1], pr.at[1], partner)
    p_n = remote(nkv, nkv_in, ps.at[2], pr.at[2], partner)
    p_k.start()
    p_v.start()

    c_wk.wait()
    keys = project(1)
    c_wv.wait()
    values = project(2)
    nkv[...] = jnp.concatenate([keys[:rows], values[:rows]], axis=1)
    p_n.start()

    def forward(d):
        q_z_in(d).wait_recv()
        for e in range(1, Y):
            q_y(Z - d, e).start()

    def split_heads(raw, which, out):
        tmp[...] = raw[which].astype(jnp.float32)
        for h in range(2):
            out[h, pl.ds(which * npos, npos), :] = tmp[
                pl.ds(h, npos, stride=2), :
            ].astype(jnp.bfloat16)

    c_pk.wait()
    split_heads(kraw, 0, kd)
    c_pv.wait()
    split_heads(vraw, 0, vd)

    for d in zorder[:2]:
        forward(d)

    c_ck.wait()
    c_cv.wait()
    c_hg.wait()
    head_gain = hg_v[...]
    row_id = lax.broadcasted_iota(jnp.int32, (16, 128), 0)
    lane_id = lax.broadcasted_iota(jnp.int32, (16, 128), 1)
    first_head = (row_id & 3) < 2
    own_half = (lane_id >= 64) == ((row_id & 1) == 1)

    def by_head(m):
        m = m[rows:].astype(jnp.float32)
        return jnp.where(first_head, m[:, :128], m[:, 128:])

    dq = jnp.where(own_half, by_head(queries), 0.0)
    own_score = jnp.sum(dq * by_head(keys), axis=-1, keepdims=True)
    scores = lax.dot_general(
        dq.astype(jnp.bfloat16), ck_v[...], NT, preferred_element_type=jnp.float32
    )
    slots = scores.shape[1]
    s_row = lax.broadcasted_iota(jnp.int32, (16, slots), 0)
    s_col = lax.broadcasted_iota(jnp.int32, (16, slots), 1)
    head_ok = (s_col & 1) == ((s_row >> 1) & 1)
    scores = jnp.where(head_ok & (s_col < 2 * length[0]), scores, -jnp.inf)
    d_max = jnp.maximum(jnp.max(scores, axis=-1, keepdims=True), own_score)
    weights = jnp.exp(scores - d_max)
    own_weight = jnp.exp(own_score - d_max)
    d_tot = jnp.sum(weights, axis=-1, keepdims=True) + own_weight
    mixed = jnp.dot(weights.astype(jnp.bfloat16), cv_v[...], preferred_element_type=jnp.float32)
    mixed = mixed + own_weight.astype(jnp.bfloat16).astype(jnp.float32) * by_head(values)
    mixed = mixed / d_tot

    def head_norm(a):
        return a * lax.rsqrt(jnp.mean(a * a, axis=-1, keepdims=True) + EPS) * head_gain

    d_heads = []
    for h in range(2):
        att = mixed[2 * h : 2 * h + 1] - lam[h] * mixed[2 * h + 1 : 2 * h + 2]
        d_heads.append(jnp.broadcast_to(head_norm(att), (16, 128)))
    dbuf[0] = jnp.concatenate(d_heads, axis=1).astype(jnp.bfloat16)

    def h_copy(buf, ss, rs, d):
        return remote(buf.at[0], buf.at[d], ss.at[d], rs.at[d], xdev(mod(tp + d, X)))

    for d in range(1, X):
        h_copy(dbuf, ds, dr, d).start()

    for d in zorder[2:]:
        forward(d)

    zeros = jnp.zeros((96, 128), jnp.bfloat16)
    p_n.wait_recv()
    for h in range(2):
        for out, base in ((kd, 0), (vd, 256)):
            cols = slice(base + h * 128, base + (h + 1) * 128)
            out[h, 2 * npos : 2 * npos + 16, :] = nkv[:, cols]
            out[h, 2 * npos + 16 : 2 * npos + 32, :] = nkv_in[:, cols]
            out[h, 2 * npos + 32 :, :] = zeros
    p_k.wait_recv()
    split_heads(kraw, 1, kd)
    p_v.wait_recv()
    split_heads(vraw, 1, vd)

    block = Y * 16
    st_lane = lax.broadcasted_iota(jnp.int32, (8, 128), 1)
    q_row = lax.broadcasted_iota(jnp.int32, (4 * block, 128), 0)
    q_lane = lax.broadcasted_iota(jnp.int32, (4 * block, 128), 1)
    in_pair = lax.rem(q_row, 2 * block)
    second = in_pair >= block
    in_block = lax.rem(in_pair, block)
    q_y_of = lax.div(in_block, 16)
    q_i = lax.rem(in_block, 16)
    key_core = jnp.where(q_lane < 16, core, 1 - core)
    key_pos = chip * 32 + key_core * 16 + lax.rem(q_lane, 16)

    def offsets(k):
        return lax.rem(Z - k, Z), k + 1

    def y_copies(k, d):
        to = mod(y + d, Y)
        who = dev(z, to)
        return (
            remote(ysend.at[k, to], yrecv.at[k, d], yds.at[k, d], ydr.at[k, d], who),
            remote(ysst.at[k, to], yrst.at[k, d], yss.at[k, d], ysr.at[k, d], who),
        )

    def chunk(k):
        oa, ob = offsets(k)
        za, zb = mod(z + oa, Z), mod(z + ob, Z)
        for e in range(1, Y):
            q_y_in(oa, e).wait_recv()
            q_y_in(ob, e).wait_recv()
        q = jnp.concatenate(
            [qbuf[za].reshape(block, 256), qbuf[zb].reshape(block, 256)], axis=0
        )
        z_of = jnp.where(second, zb, za)
        q_pos = (z_of * Y + q_y_of) * 32 + core * 16 + q_i
        visible = (key_pos <= q_pos) & (q_lane < 32)
        lane2 = lax.broadcasted_iota(jnp.int32, (2 * block, 128), 1)
        stats = [jnp.zeros((8, 128), jnp.float32) for _ in range(Y)]
        for h in range(2):
            qh = q[:, h * 128 : (h + 1) * 128]
            zero = jnp.zeros_like(qh)
            stacked = jnp.concatenate(
                [jnp.where(lane2 < 64, qh, zero), jnp.where(lane2 < 64, zero, qh)], axis=0
            )
            s = lax.dot_general(stacked, kd[h], NT, preferred_element_type=jnp.float32)
            s = jnp.concatenate(
                [s[:, : 2 * npos], jnp.where(visible, s[:, 2 * npos :], -jnp.inf)], axis=1
            )
            top = jnp.max(s, axis=-1, keepdims=True)
            w = jnp.exp(s - top)
            tot = jnp.sum(w, axis=-1, keepdims=True)
            acc = jnp.dot(
                w.astype(jnp.bfloat16), vd[h], preferred_element_type=jnp.float32
            ).astype(jnp.bfloat16)
            for m in range(2):
                combo = 2 * h + m
                for zi in range(2):
                    for yy in range(Y):
                        base = m * 2 * block + zi * block + yy * 16
                        ysend[k, yy, zi * 16 : zi * 16 + 16, combo * 128 : (combo + 1) * 128] = (
                            acc[base : base + 16]
                        )
                        for half in range(2):
                            lane = zi * 8 + half * 4 + combo
                            r0 = base + half * 8
                            stats[yy] = jnp.where(st_lane == lane, top[r0 : r0 + 8], stats[yy])
                            stats[yy] = jnp.where(
                                st_lane == lane + 64, tot[r0 : r0 + 8], stats[yy]
                            )
        for yy in range(Y):
            ysst[k, yy] = stats[yy]
        for d in range(1, Y):
            for copy in y_copies(k, d):
                copy.start()

    def merged(stats, blocks, zi):
        top = functools.reduce(jnp.maximum, stats)
        scale = [jnp.exp(s - top) for s in stats]
        total = sum(pltpu.roll(f, 64, 1) * s for f, s in zip(scale, stats))
        outs = []
        for combo in range(4):
            lane = zi * 8 + combo
            acc = None
            for f, b in zip(scale, blocks):
                col = jnp.concatenate([f[:, lane : lane + 1], f[:, lane + 4 : lane + 5]], axis=0)
                term = col * b(combo)
                acc = term if acc is None else acc + term
            outs.append(acc)
        return top, total, outs

    def z_copies(k, zi):
        o = offsets(k)[zi]
        who = dev(mod(z + o, Z), y)
        return (
            remote(zsend.at[k, zi], zrecv.at[k, zi], zds.at[k, zi], zdr.at[k, zi], who),
            remote(zsst.at[k], zrst.at[k, zi], zss.at[k, zi], zsr.at[k, zi], who),
        )

    def combine(k):
        for d in range(1, Y):
            for copy in y_copies(k, d):
                copy.wait_recv()
        stats = [ysst[k, y]] + [yrst[k, d] for d in range(1, Y)]
        for zi in range(2):
            blocks = []
            for d in range(Y):
                src = ysend[k, y, zi * 16 : zi * 16 + 16, :] if d == 0 else yrecv[
                    k, d, zi * 16 : zi * 16 + 16, :
                ]
                blocks.append(
                    lambda c, src=src: src[:, c * 128 : (c + 1) * 128].astype(jnp.float32)
                )
            top, total, outs = merged(stats, blocks, zi)
            zsend[k, zi] = jnp.concatenate(outs, axis=1).astype(jnp.bfloat16)
            if zi == 0:
                zsst[k] = jnp.where(st_lane < 64, top, total)
        for copy in z_copies(k, 1):
            copy.start()

        @pl.when(k > 0)
        def _():
            for copy in z_copies(k, 0):
                copy.start()

    @pl.loop(0, pairs + LAG)
    def _(it):
        @pl.when(it < pairs)
        def _():
            chunk(it)

        @pl.when(it >= LAG)
        def _():
            combine(it - LAG)

    for k in range(pairs):
        for zi in range(2):
            if (k, zi) != (0, 0):
                for copy in z_copies(k, zi):
                    copy.wait_recv()
    stats, blocks = [], []
    for k in range(pairs):
        for zi in range(2):
            own = (k, zi) == (0, 0)
            s = zsst[0] if own else zrst[k, zi]
            if zi == 1:
                s = pltpu.roll(s, 120, 1)
            stats.append(s)
            src = zsend[0, 0] if own else zrecv[k, zi]
            blocks.append(lambda c, src=src: src[:, c * 128 : (c + 1) * 128].astype(jnp.float32))
    _, total, outs = merged(stats, blocks, 0)
    tot_cols = [
        jnp.concatenate([total[:, 64 + c : 65 + c], total[:, 68 + c : 69 + c]], axis=0)
        for c in range(4)
    ]
    p_heads = []
    for h in range(2):
        one = outs[2 * h] / tot_cols[2 * h]
        two = outs[2 * h + 1] / tot_cols[2 * h + 1]
        p_heads.append(head_norm(one - lam[h] * two))
    hbuf[0] = jnp.concatenate(p_heads, axis=1).astype(jnp.bfloat16)
    for d in range(1, X):
        h_copy(hbuf, hs, hr, d).start()

    c_wo.wait()
    total_out = None
    for d in range(X):
        if d > 0:
            h_copy(hbuf, hs, hr, d).wait_recv()
            h_copy(dbuf, ds, dr, d).wait_recv()
        src = mod(tp + X - d, X)
        lhs = jnp.concatenate([hbuf[d], dbuf[d]], axis=0)
        part = jnp.dot(
            lhs, wo_v[pl.ds(pl.multiple_of(src * 256, 256), 256), :],
            preferred_element_type=jnp.float32,
        )
        total_out = part if total_out is None else total_out + part
    out_p[...] = total_out[:rows].astype(jnp.bfloat16)
    out_d[...] = total_out[rows : rows + 1].astype(jnp.bfloat16)

    for d in range(1, Z):
        q_z(d).wait_send()
    for o in range(Z):
        for e in range(1, Y):
            q_y(o, e).wait_send()
    for copy in (p_k, p_v, p_n):
        copy.wait_send()
    for k in range(pairs):
        for d in range(1, Y):
            for copy in y_copies(k, d):
                copy.wait_send()
        for zi in range(2):
            if (k, zi) != (0, 0):
                for copy in z_copies(k, zi):
                    copy.wait_send()
    for d in range(1, X):
        h_copy(hbuf, hs, hr, d).wait_send()
        h_copy(dbuf, ds, dr, d).wait_send()


def shards(Z, Y, X, *args):
    (x, xd, gain, wq, wk, wv, wo, hg, lam, pk, pv, ck, cv, lengths) = args
    D = x.shape[1]
    npos = pk.shape[0]
    slots = ck.shape[1]
    pairs = Z // 2
    bf, f32 = jnp.bfloat16, jnp.float32
    any_ = pl.BlockSpec(memory_space=pl.ANY)
    smem = pl.BlockSpec(memory_space=pltpu.SMEM)
    vmem = pl.BlockSpec(memory_space=pltpu.VMEM)
    V, S = pltpu.VMEM, pltpu.SemaphoreType.DMA
    out_cols = wo.shape[1]
    scratch = [
        V((16, D), bf), V((1, D), bf), V((1, D), f32), V((1, 128), f32),
        V((3, D, 256), bf), V(wo.shape, bf),
        V((2, 2 * npos, 128), bf), V((2, 2 * npos, 128), bf),
        V((2, 2 * npos + 128, 128), bf), V((2, 2 * npos + 128, 128), bf),
        V((2 * slots, 128), bf), V((2 * slots, 128), bf), V((2 * npos, 128), f32),
        V((16, 512), bf), V((16, 512), bf),
        V((Z, Y, 16, 256), bf),
        V((pairs, Y, 32, 512), bf), V((pairs, Y, 8, 128), f32),
        V((pairs, Y, 32, 512), bf), V((pairs, Y, 8, 128), f32),
        V((pairs, 2, 16, 512), bf), V((pairs, 8, 128), f32),
        V((pairs, 2, 16, 512), bf), V((pairs, 2, 8, 128), f32),
        V((X, 16, 256), bf), V((X, 16, 256), bf),
        S((12,)), S((3,)), S((3,)), S((Z,)), S((Z,)), S((Z, Y)), S((Z, Y)),
        S((pairs, Y)), S((pairs, Y)), S((pairs, Y)), S((pairs, Y)),
        S((pairs, 2)), S((pairs, 2)), S((pairs, 2)), S((pairs, 2)),
        S((X,)), S((X,)), S((X,)), S((X,)),
    ]
    return pl.pallas_call(
        functools.partial(kernel, Z, Y, X),
        out_shape=(
            jax.ShapeDtypeStruct((16, out_cols), bf),
            jax.ShapeDtypeStruct((1, out_cols), bf),
        ),
        in_specs=[any_] * 8 + [smem] + [any_] * 4 + [smem],
        out_specs=(vmem, vmem),
        scratch_shapes=scratch,
        compiler_params=pltpu.CompilerParams(collective_id=0, has_side_effects=True),
    )(
        x, xd, gain.reshape(1, D), wq, wk, wv, wo, hg.reshape(1, 128), lam,
        pk.reshape(2 * npos, 128), pv.reshape(2 * npos, 128),
        ck.reshape(2 * slots, 128), cv.reshape(2 * slots, 128), lengths,
    )


def solution(mesh):
    kv, X = mesh.shape["kv"], mesh.shape["tp"]
    Y = 4 if kv == 64 else 2
    Z = kv // (2 * Y)
    placed = (
        P("kv", None),
        P("kv", None),
        P(),
        P(None, "tp"),
        P(None, "tp"),
        P(None, "tp"),
        P(None, "tp"),
        P(),
        P("tp"),
        P("kv", "tp", None),
        P("kv", "tp", None),
        P("kv", None, "tp", None),
        P("kv", None, "tp", None),
        P("kv"),
    )
    return jax.shard_map(
        functools.partial(shards, Z, Y, X),
        mesh=mesh,
        in_specs=placed,
        out_specs=(P("kv", "tp"), P("kv", "tp")),
        check_vma=False,
    )
```

time: 148 us -> 45.1 us (0.30); the launches traced: 146 us -> 44.9 us
  Pallas kernels: 0 us -> 41.7 us
  local copies, waits for them, and re-layouts: 37.1 us -> 1.91 us
  waiting for transfers between devices: 30.1 us -> 0 us
  starting transfers between devices: 27.6 us -> 0 us
  other arithmetic: 20.6 us -> 0 us
  matrix products: 19.6 us -> 0 us
  blocking collectives: 8.7 us -> 0 us
    pallas_call x0 -> x1, Pallas kernels: none -> 41.7 us  [shards(): pl.pallas_call(functools.partial(kernel, Z, Y, X), out_shape=(jax.ShapeDt...]
    all_to_all x3 -> x0, waiting for transfers between devices: 30.1 us -> none  [the longest x2 30.1 us: side_by_side(): lax.all_to_all(both, axis, split_axis=split_dim, concat_axis=concat_dim,...]
    all_to_all x3 -> x0, starting transfers between devices: 27.6 us -> none  [the longest x2 15.2 us: side_by_side(): lax.all_to_all(both, axis, split_axis=split_dim, concat_axis=concat_dim,...]
    dot_general x16 -> x0, matrix products: 19.6 us -> none  [the longest x4 7.99 us: block_terms(): jnp.einsum('hqk,khd->qhd', weights.astype(jnp.bfloat16), values_all, pref...]
    dynamic_update_slice x10 -> x0, local copies, waits for them, and re-layouts: 9.45 us -> none  [shards(): lax.map(lambda inputs: block_terms(inputs[0], inputs[1]), (blocks, starts))]
    all_to_all x1 -> x0, blocking collectives: 8.7 us -> none  [sent_to_all(): lax.all_to_all(jnp.broadcast_to(array[None], (length, *array.shape)), axi...]
    reduce_sum x7 -> x0, other arithmetic: 7.5 us -> none  [the longest x1 3.94 us: shards(): jnp.sum(value_factor * weighted, axis=0)]
    dynamic_slice x6 -> x0, local copies, waits for them, and re-layouts: 6.17 us -> none  [shards(): lax.map(lambda inputs: block_terms(inputs[0], inputs[1]), (blocks, starts))]
  transfers between devices with their start and end apart: 3 -> 0, of which waited for: 2 -> 0; matrix products, arithmetic and copies ran while one was open for 17% -> 0% of each run, Pallas kernels for 0% -> 0%
where the time goes in v1:
time: 45.1 us; the launch traced here: 44.9 us
  Pallas kernels  41.7 us (92%)
  local copies, waits for them, and re-layouts  1.91 us (4%)
  between operations  1.3 us (3%)
    pallas_call x1, Pallas kernels, shards(): pl.pallas_call(functools.partial(kernel, Z, Y, X), out_shape=(jax.ShapeDt...  41.7 us
    unnamed x4, local copies, waits for them, and re-layouts  1.91 us

profile of v1, /device:TPU:2, one launch (start us, length us, event | category | flops | bytes accessed | tf_op | source)
XLA Modules:
  0.0 44.9 jit_solution(10171106657744051727)
XLA Ops:
  1.3 41.7 %shard_map.149 = (bf16[16,512]{1,0:T(8,128)(2,1)}, bf16[1,512]{1,0:T(2,128)(2,1)}) custom-call(bf16[16,2048]{1,0:T(8,128)(2,1)} %x_hbm.1, bf16[1,2048]{1,0:T(2,128)(2,1)} %xd_hbm.1, f32[1,2048]{1,0:T(1,128)} %bitcast.10, bf16[2048,256]{1,0:T(8,128)(2,1)} %wq_hbm.1, bf16[2048,256]{1,0:T(8,128)(2,1)} %wk_hbm.1, bf16[2048,256]{1,0:T(8,128)(2,1)} %wv_hbm.1, ...), custom_call_target="tpu_custom_call" | custom-call | tf_op jit(solution)/shard_map/pallas_call | solution.py:455
  43.0 0.0 copy-start
  43.0 1.3 %copy.19 = bf16[16,512]{1,0:T(8,128)(2,1)} copy(bf16[16,512]{1,0:T(8,128)(2,1)} %get-tuple-element.4) | data formatting | bytes 32768
  44.3 0.0 copy-done
  44.3 0.6 %copy.20 = bf16[1,512]{1,0:T(2,128)(2,1)} copy(bf16[1,512]{1,0:T(2,128)(2,1)S(1)} %copy-done) | data formatting | bytes 2048
Async XLA Ops:
  43.0 1.3 %copy-start = (bf16[1,512]{1,0:T(2,128)(2,1)S(1)}, bf16[1,512]{1,0:T(2,128)(2,1)}, u32[]{:S(2)}) copy-start(bf16[1,512]{1,0:T(2,128)(2,1)} %get-tuple-element.5) | copy-start | bytes 3076

commit v2 on v1

v2 whole, which is shorter than its diff:
```python
import functools

import jax
import jax.numpy as jnp
from jax import lax
from jax.experimental import pallas as pl
from jax.experimental.pallas import tpu as pltpu
from jax.sharding import PartitionSpec as P

EPS = 1e-06
MESH = pl.DeviceIdType.MESH
NT = (((1,), (1,)), ((), ()))
LAG = 4


def kernel(
    Z, Y, X,
    x_hbm, xd_hbm, gain_hbm, wq_hbm, wk_hbm, wv_hbm, wo_hbm, hg_hbm, lam_hbm, pk_hbm, pv_hbm,
    ck_hbm, cv_hbm, len_hbm,
    out_ref,
    x_v, xd_v, gain_v, hg_v, w_v, wo_v, kraw, vraw, kd, vd, ck_v, cv_v, tmp,
    nkv, nkv_in, qbuf, ysend, yrecv, zsend, zrecv, hbuf, lam, length,
    lsem, ps, pr, qzs, qzr, qys, qyr, yds, ydr, zds, zdr, hs, hr,
):
    kv = lax.axis_index("kv")
    tp = lax.axis_index("tp")
    core = lax.rem(kv, 2)
    chip = lax.div(kv, 2)
    y = lax.rem(chip, Y)
    z = lax.div(chip, Y)
    rows = x_v.shape[0]
    npos = kraw.shape[1] // 2

    def dev(zz, yy):
        return ((zz * Y + yy) * 2 + core, tp)

    partner = (chip * 2 + 1 - core, tp)

    def xdev(xx):
        return (kv, xx)

    def mod(a, n):
        return lax.rem(a + n, n)

    barrier = pltpu.get_barrier_semaphore()
    for d in range(1, Z):
        pl.semaphore_signal(barrier, inc=1, device_id=dev(mod(z + d, Z), y), device_id_type=MESH)
    for d in range(1, Y):
        pl.semaphore_signal(barrier, inc=1, device_id=dev(z, mod(y + d, Y)), device_id_type=MESH)
    for d in range(1, X):
        pl.semaphore_signal(barrier, inc=1, device_id=xdev(mod(tp + d, X)), device_id_type=MESH)
    pl.semaphore_signal(barrier, inc=1, device_id=partner, device_id_type=MESH)

    local = []

    def fetch(src, dst):
        copy = pltpu.make_async_copy(src, dst, lsem.at[len(local)])
        copy.start()
        local.append(copy)
        return copy

    c_x = fetch(x_hbm, x_v)
    c_xd = fetch(xd_hbm, xd_v)
    c_gain = fetch(gain_hbm, gain_v)
    c_wq = fetch(wq_hbm, w_v.at[0])
    c_wk = fetch(wk_hbm, w_v.at[1])
    c_wv = fetch(wv_hbm, w_v.at[2])
    c_pk = fetch(pk_hbm, kraw.at[0])
    c_pv = fetch(pv_hbm, vraw.at[0])
    c_ck = fetch(ck_hbm, ck_v)
    c_cv = fetch(cv_hbm, cv_v)
    c_wo = fetch(wo_hbm, wo_v)
    c_hg = fetch(hg_hbm, hg_v)
    c_lam = fetch(lam_hbm, lam)
    c_len = fetch(len_hbm, length)

    def remote(src, dst, ssem, rsem, device):
        return pltpu.make_async_remote_copy(
            src_ref=src, dst_ref=dst, send_sem=ssem, recv_sem=rsem,
            device_id=device, device_id_type=MESH,
        )

    c_x.wait()
    c_xd.wait()
    c_gain.wait()
    gain = gain_v[...]

    def norm(v):
        v = v.astype(jnp.float32)
        return v * lax.rsqrt(jnp.mean(v * v, axis=-1, keepdims=True) + EPS) * gain

    normed_p = norm(x_v[...]).astype(jnp.bfloat16)
    normed_d = jnp.broadcast_to(norm(xd_v[...]), (16, x_v.shape[1])).astype(jnp.bfloat16)
    normed = jnp.concatenate([normed_p, normed_d], axis=0)

    def project(which):
        return jnp.dot(normed, w_v[which], preferred_element_type=jnp.float32).astype(jnp.bfloat16)

    c_wq.wait()
    queries = project(0) * jnp.bfloat16(0.125)
    qbuf[z, y] = queries[:rows]

    c_wk.wait()
    keys = project(1)
    c_wv.wait()
    values = project(2)
    nkv[...] = jnp.concatenate([keys[:rows], values[:rows]], axis=1)

    def split_heads(raw, which, out):
        tmp[...] = raw[which].astype(jnp.float32)
        for h in range(2):
            out[h, pl.ds(which * npos, npos), :] = tmp[
                pl.ds(h, npos, stride=2), :
            ].astype(jnp.bfloat16)

    c_pk.wait()
    split_heads(kraw, 0, kd)
    c_pv.wait()
    split_heads(vraw, 0, vd)

    pl.semaphore_wait(barrier, Z + Y + X - 2)

    def q_z(d):
        return remote(qbuf.at[z, y], qbuf.at[z, y], qzs, qzr.at[d], dev(mod(z + d, Z), y))

    def q_z_in(d):
        src = mod(z + Z - d, Z)
        return remote(qbuf.at[src, y], qbuf.at[src, y], qzs, qzr.at[d], dev(src, y))

    def q_y(o, e):
        zz = mod(z + o, Z)
        return remote(qbuf.at[zz, y], qbuf.at[zz, y], qys, qyr.at[o], dev(z, mod(y + e, Y)))

    def all_of(ref, ssem, rsem):
        return remote(ref, ref, ssem, rsem, partner)

    zorder = []
    for d in range(1, Z // 2 + 1):
        zorder.append(d)
        if Z - d not in zorder:
            zorder.append(Z - d)
    for d in reversed(zorder):
        q_z(d).start()
    for e in range(1, Y):
        q_y(0, e).start()

    p_k = remote(pk_hbm, kraw.at[1], ps.at[0], pr.at[0], partner)
    p_v = remote(pv_hbm, vraw.at[1], ps.at[1], pr.at[1], partner)
    p_n = remote(nkv, nkv_in, ps.at[2], pr.at[2], partner)
    p_n.start()
    p_k.start()
    p_v.start()

    def forward(d):
        q_z_in(d).wait_recv()
        for e in range(1, Y):
            q_y(Z - d, e).start()

    zeros = jnp.zeros((96, 128), jnp.bfloat16)
    p_n.wait_recv()
    for h in range(2):
        for out, base in ((kd, 0), (vd, 256)):
            cols = slice(base + h * 128, base + (h + 1) * 128)
            out[h, 2 * npos : 2 * npos + 16, :] = nkv[:, cols]
            out[h, 2 * npos + 16 : 2 * npos + 32, :] = nkv_in[:, cols]
            out[h, 2 * npos + 32 :, :] = zeros
    p_k.wait_recv()
    split_heads(kraw, 1, kd)
    p_v.wait_recv()
    split_heads(vraw, 1, vd)

    for d in zorder:
        forward(d)

    c_hg.wait()
    c_lam.wait()
    c_len.wait()
    head_gain = hg_v[...]

    def head_norm(a):
        return a * lax.rsqrt(jnp.mean(a * a, axis=-1, keepdims=True) + EPS) * head_gain

    def h_copy(part, d):
        at = pl.ds(16 * part, 16)
        return remote(hbuf.at[0, at], hbuf.at[d, at], hs, hr, xdev(mod(tp + d, X)))

    def decode():
        c_ck.wait()
        c_cv.wait()
        row_id = lax.broadcasted_iota(jnp.int32, (16, 128), 0)
        lane_id = lax.broadcasted_iota(jnp.int32, (16, 128), 1)
        first_head = (row_id & 3) < 2
        own_half = (lane_id >= 64) == ((row_id & 1) == 1)

        def by_head(m):
            m = m[rows:].astype(jnp.float32)
            return jnp.where(first_head, m[:, :128], m[:, 128:])

        dq = jnp.where(own_half, by_head(queries), 0.0)
        own_score = jnp.sum(dq * by_head(keys), axis=-1, keepdims=True)
        scores = lax.dot_general(
            dq.astype(jnp.bfloat16), ck_v[...], NT, preferred_element_type=jnp.float32
        )
        slots = scores.shape[1]
        s_row = lax.broadcasted_iota(jnp.int32, (16, slots), 0)
        s_col = lax.broadcasted_iota(jnp.int32, (16, slots), 1)
        head_ok = (s_col & 1) == ((s_row >> 1) & 1)
        scores = jnp.where(head_ok & (s_col < 2 * length[0]), scores, -jnp.inf)
        d_max = jnp.maximum(jnp.max(scores, axis=-1, keepdims=True), own_score)
        weights = jnp.exp(scores - d_max)
        own_weight = jnp.exp(own_score - d_max)
        d_tot = jnp.sum(weights, axis=-1, keepdims=True) + own_weight
        mixed = jnp.dot(weights.astype(jnp.bfloat16), cv_v[...], preferred_element_type=jnp.float32)
        mixed = mixed + own_weight.astype(jnp.bfloat16).astype(jnp.float32) * by_head(values)
        mixed = mixed / d_tot

        d_heads = []
        for h in range(2):
            att = mixed[2 * h : 2 * h + 1] - lam[h] * mixed[2 * h + 1 : 2 * h + 2]
            d_heads.append(jnp.broadcast_to(head_norm(att), (16, 128)))
        hbuf[0, 16:, :] = jnp.concatenate(d_heads, axis=1).astype(jnp.bfloat16)

        for d in range(1, X):
            h_copy(1, d).start()

    block = Y * 16
    st_lane = lax.broadcasted_iota(jnp.int32, (16, 128), 1)
    q_row = lax.rem(lax.broadcasted_iota(jnp.int32, (2 * block, 128), 0), block)
    q_lane = lax.broadcasted_iota(jnp.int32, (2 * block, 128), 1)
    q_off = lax.div(q_row, 16) * 32 + core * 16 + lax.rem(q_row, 16)
    key_core = jnp.where(q_lane < 16, core, 1 - core)
    key_pos = chip * 32 + key_core * 16 + lax.rem(q_lane, 16)
    lane1 = lax.broadcasted_iota(jnp.int32, (block, 128), 1)

    def offset(k):
        half = lax.div(k + 1, 2)
        return jnp.where(lax.rem(k, 2) == 1, half, lax.rem(Z - half, Z))

    def packed(stat):
        high = stat.astype(jnp.bfloat16).astype(jnp.float32)
        rest = stat - high
        middle = rest.astype(jnp.bfloat16).astype(jnp.float32)
        low = rest - middle
        return (high + pltpu.roll(middle, 16, 1) + pltpu.roll(low, 32, 1)).astype(jnp.bfloat16)

    def unpacked(tile):
        tile = tile.astype(jnp.float32)
        return tile + pltpu.roll(tile, 112, 1) + pltpu.roll(tile, 96, 1)

    def y_copy(k, d):
        to = mod(y + d, Y)
        return remote(ysend.at[k, to], yrecv.at[k, d - 1], yds, ydr.at[k], dev(z, to))

    def chunk(k):
        o = offset(k)
        zz = mod(z + o, Z)
        all_of(qbuf.at[zz, pl.ds(0, Y - 1)], qys, qyr.at[o]).wait_recv()
        q = qbuf[zz].reshape(block, 256)
        visible = (key_pos <= zz * (Y * 32) + q_off) & (q_lane < 32)
        stats = jnp.zeros((block, 128), jnp.float32)
        for h in range(2):
            qh = q[:, h * 128 : (h + 1) * 128]
            zero = jnp.zeros_like(qh)
            stacked = jnp.concatenate(
                [jnp.where(lane1 < 64, qh, zero), jnp.where(lane1 < 64, zero, qh)], axis=0
            )
            s = lax.dot_general(stacked, kd[h], NT, preferred_element_type=jnp.float32)
            s = jnp.concatenate(
                [s[:, : 2 * npos], jnp.where(visible, s[:, 2 * npos :], -jnp.inf)], axis=1
            )
            top = jnp.max(s, axis=-1, keepdims=True)
            w = jnp.exp(s - top)
            tot = jnp.sum(w, axis=-1, keepdims=True)
            acc = jnp.dot(
                w.astype(jnp.bfloat16), vd[h], preferred_element_type=jnp.float32
            ).astype(jnp.bfloat16)
            for m in range(2):
                combo = 2 * h + m
                of_map = slice(m * block, (m + 1) * block)
                stats = jnp.where(lane1 == combo, top[of_map], stats)
                stats = jnp.where(lane1 == combo + 64, tot[of_map], stats)
                for yy in range(Y):
                    base = m * block + yy * 16
                    ysend[k, yy, :, combo * 128 : (combo + 1) * 128] = acc[base : base + 16]
        stats = packed(stats)
        for yy in range(Y):
            ysend[k, yy, :, 512:] = stats[yy * 16 : yy * 16 + 16]
        for d in range(1, Y):
            y_copy(k, d).start()

    def merged(sources):
        stats = [unpacked(data[:, 512:]) for data in sources]
        top = functools.reduce(jnp.maximum, stats)
        scale = [jnp.exp(s - top) for s in stats]
        total = sum(pltpu.roll(f, 64, 1) * s for f, s in zip(scale, stats))
        outs = []
        for combo in range(4):
            acc = None
            for f, data in zip(scale, sources):
                term = f[:, combo : combo + 1] * data[
                    :, combo * 128 : (combo + 1) * 128
                ].astype(jnp.float32)
                acc = term if acc is None else acc + term
            outs.append(acc)
        return top, total, outs

    def z_copy(k):
        return remote(zsend.at[k], zrecv.at[k], zds, zdr, dev(mod(z + offset(k), Z), y))

    def combine(k):
        all_of(yrecv.at[k], yds, ydr.at[k]).wait_recv()
        top, total, outs = merged([ysend.at[k, y]] + [yrecv.at[k, i] for i in range(Y - 1)])
        for c in range(4):
            zsend[k, :, c * 128 : (c + 1) * 128] = outs[c].astype(jnp.bfloat16)
        totals = jnp.where((st_lane >= 64) & (st_lane < 68), total, 0.0)
        zsend[k, :, 512:] = packed(jnp.where(st_lane < 4, top, totals))

        @pl.when(k > 0)
        def _():
            z_copy(k).start()

    @pl.loop(0, Z + LAG)
    def _(it):
        @pl.when(it < Z)
        def _():
            chunk(it)

        @pl.when(it == Z - 1)
        def _():
            decode()

        @pl.when(it >= LAG)
        def _():
            combine(it - LAG)

    zall = all_of(zrecv.at[pl.ds(1, Z - 1)], zds, zdr)
    zall.wait_recv()
    _, total, outs = merged([zsend.at[0]] + [zrecv.at[k] for k in range(1, Z)])
    tot_cols = [total[:, 64 + c : 65 + c] for c in range(4)]
    p_heads = []
    for h in range(2):
        one = outs[2 * h] / tot_cols[2 * h]
        two = outs[2 * h + 1] / tot_cols[2 * h + 1]
        p_heads.append(head_norm(one - lam[h] * two))
    hbuf[0, :16, :] = jnp.concatenate(p_heads, axis=1).astype(jnp.bfloat16)
    for d in range(1, X):
        h_copy(0, d).start()

    c_wo.wait()

    def out_term(d):
        src = mod(tp + X - d, X)
        return jnp.dot(
            hbuf[d], wo_v[pl.ds(pl.multiple_of(src * 256, 256), 256), :],
            preferred_element_type=jnp.float32,
        )

    total_out = out_term(0)
    if X > 1:
        all_of(hbuf.at[pl.ds(1, X - 1)], hs, hr).wait_recv()
    for d in range(1, X):
        total_out = total_out + out_term(d)
    out_ref[...] = total_out.astype(jnp.bfloat16)

    all_of(qbuf.at[pl.ds(0, Z - 1), 0], qzs, qzr.at[0]).wait_send()
    all_of(qbuf.at[:, pl.ds(0, Y - 1)], qys, qyr.at[0]).wait_send()
    for copy in (p_k, p_v, p_n):
        copy.wait_send()
    all_of(ysend.at[:, pl.ds(0, Y - 1)], yds, ydr.at[0]).wait_send()
    zall.wait_send()
    if X > 1:
        all_of(hbuf.at[pl.ds(1, X - 1)], hs, hr).wait_send()


def shards(Z, Y, X, *args):
    (x, xd, gain, wq, wk, wv, wo, hg, lam, pk, pv, ck, cv, lengths) = args
    D = x.shape[1]
    npos = pk.shape[0]
    slots = ck.shape[1]
    bf, f32 = jnp.bfloat16, jnp.float32
    any_ = pl.BlockSpec(memory_space=pl.ANY)
    vmem = pl.BlockSpec(memory_space=pltpu.VMEM)
    V, S = pltpu.VMEM, pltpu.SemaphoreType.DMA
    out_cols = wo.shape[1]
    scratch = [
        V((16, D), bf), V((1, D), bf), V((1, D), f32), V((1, 128), f32),
        V((3, D, 256), bf), V(wo.shape, bf),
        V((2, 2 * npos, 128), bf), V((2, 2 * npos, 128), bf),
        V((2, 2 * npos + 128, 128), bf), V((2, 2 * npos + 128, 128), bf),
        V((2 * slots, 128), bf), V((2 * slots, 128), bf), V((2 * npos, 128), f32),
        V((16, 512), bf), V((16, 512), bf),
        V((Z, Y, 16, 256), bf),
        V((Z, Y, 16, 640), bf), V((Z, Y - 1, 16, 640), bf),
        V((Z, 16, 640), bf), V((Z, 16, 640), bf), V((X, 32, 256), bf),
        pltpu.SMEM((2,), f32), pltpu.SMEM((1,), jnp.int32),
        S((14,)), S((3,)), S((3,)), S, S((Z,)), S, S((Z,)), S, S((Z,)), S, S, S, S,
    ]
    out = pl.pallas_call(
        functools.partial(kernel, Z, Y, X),
        out_shape=jax.ShapeDtypeStruct((32, out_cols), bf),
        in_specs=[any_] * 14,
        out_specs=vmem,
        scratch_shapes=scratch,
        compiler_params=pltpu.CompilerParams(collective_id=0, has_side_effects=True),
    )(
        x, xd, gain.reshape(1, D), wq, wk, wv, wo, hg.reshape(1, 128), lam,
        pk.reshape(2 * npos, 128), pv.reshape(2 * npos, 128),
        ck.reshape(2 * slots, 128), cv.reshape(2 * slots, 128), lengths,
    )
    return out[:16], out[16:17]


def solution(mesh):
    kv, X = mesh.shape["kv"], mesh.shape["tp"]
    Y = 4
    Z = kv // (2 * Y)
    placed = (
        P("kv", None),
        P("kv", None),
        P(),
        P(None, "tp"),
        P(None, "tp"),
        P(None, "tp"),
        P(None, "tp"),
        P(),
        P("tp"),
        P("kv", "tp", None),
        P("kv", "tp", None),
        P("kv", None, "tp", None),
        P("kv", None, "tp", None),
        P("kv"),
    )
    return jax.shard_map(
        functools.partial(shards, Z, Y, X),
        mesh=mesh,
        in_specs=placed,
        out_specs=(P("kv", "tp"), P("kv", "tp")),
        check_vma=False,
    )
```

time: 45.1 us -> 42 us (0.931)
  Pallas kernels: 41.7 us -> 37.8 us
  local copies, waits for them, and re-layouts: 1.91 us -> 2.6 us
    pallas_call x1, Pallas kernels: 41.7 us -> 37.8 us  [shards(): pl.pallas_call(functools.partial(kernel, Z, Y, X), out_shape=jax.ShapeDty...]
    slice x0 -> x2, local copies, waits for them, and re-layouts: none -> 2.6 us  [shards(): return (out[:16], out[16:17])]
    unnamed x4 -> x0, local copies, waits for them, and re-layouts: 1.91 us -> none
where the time goes in v2:
time: 42 us; the launch traced here: 41.7 us
  Pallas kernels  37.8 us (90%)
  local copies, waits for them, and re-layouts  2.6 us (6%)
  between operations  1.29 us (3%)
    pallas_call x1, Pallas kernels, shards(): pl.pallas_call(functools.partial(kernel, Z, Y, X), out_shape=jax.ShapeDty...  37.8 us
    slice x2, local copies, waits for them, and re-layouts, shards(): return (out[:16], out[16:17])  2.6 us

profile of v2, /device:TPU:2, one launch (start us, length us, event | category | flops | bytes accessed | tf_op | source)
XLA Modules:
  0.0 41.7 jit_solution(3116605040619025654)
XLA Ops:
  1.3 37.8 %shard_map.149 = bf16[32,512]{1,0:T(8,128)(2,1)} custom-call(bf16[16,2048]{1,0:T(8,128)(2,1)} %x_hbm.1, bf16[1,2048]{1,0:T(2,128)(2,1)} %xd_hbm.1, f32[1,2048]{1,0:T(1,128)} %bitcast.10, bf16[2048,256]{1,0:T(8,128)(2,1)} %wq_hbm.1, bf16[2048,256]{1,0:T(8,128)(2,1)} %wk_hbm.1, bf16[2048,256]{1,0:T(8,128)(2,1)} %wv_hbm.1, bf16[1024,512]{1,0:T(8,128)(2,1)} %wo_hbm.1, ...), custom_call_target="tpu_custom_call" | custom-call | tf_op jit(solution)/shard_map/pallas_call | solution.py:398
  39.1 1.3 %slice.7 = bf16[1,512]{1,0:T(2,128)(2,1)} slice(bf16[32,512]{1,0:T(8,128)(2,1)} %shard_map.149), slice={[16:17], [0:512]} | slice | bytes 2048 | tf_op jit(solution)/shard_map/slice | solution.py:410
  40.4 1.3 %slice.6 = bf16[16,512]{1,0:T(8,128)(2,1)} slice(bf16[32,512]{1,0:T(8,128)(2,1)} %shard_map.149), slice={[0:16], [0:512]} | slice | bytes 32768 | tf_op jit(solution)/shard_map/slice | solution.py:410

commit v3 on v2

--- a/solution.py
+++ b/solution.py
@@ -225,12 +225,12 @@
 
     block = Y * 16
     st_lane = lax.broadcasted_iota(jnp.int32, (16, 128), 1)
-    q_row = lax.rem(lax.broadcasted_iota(jnp.int32, (2 * block, 128), 0), block)
-    q_lane = lax.broadcasted_iota(jnp.int32, (2 * block, 128), 1)
+    q_row = lax.broadcasted_iota(jnp.int32, (block, 128), 0)
+    q_lane = lax.broadcasted_iota(jnp.int32, (block, 128), 1)
     q_off = lax.div(q_row, 16) * 32 + core * 16 + lax.rem(q_row, 16)
     key_core = jnp.where(q_lane < 16, core, 1 - core)
     key_pos = chip * 32 + key_core * 16 + lax.rem(q_lane, 16)
-    lane1 = lax.broadcasted_iota(jnp.int32, (block, 128), 1)
+    lane1 = lax.broadcasted_iota(jnp.int32, (2 * block, 128), 1)
 
     def offset(k):
         half = lax.div(k + 1, 2)
@@ -249,15 +249,25 @@
 
     def y_copy(k, d):
         to = mod(y + d, Y)
-        return remote(ysend.at[k, to], yrecv.at[k, d - 1], yds, ydr.at[k], dev(z, to))
-
-    def chunk(k):
-        o = offset(k)
-        zz = mod(z + o, Z)
-        all_of(qbuf.at[zz, pl.ds(0, Y - 1)], qys, qyr.at[o]).wait_recv()
-        q = qbuf[zz].reshape(block, 256)
-        visible = (key_pos <= zz * (Y * 32) + q_off) & (q_lane < 32)
-        stats = jnp.zeros((block, 128), jnp.float32)
+        return remote(ysend.at[k + 1, to], yrecv.at[k, d - 1], yds, ydr.at[k], dev(z, to))
+
+    def blocks_of(it):
+        return [2 * it - 1, 2 * it]
+
+    def chunk(it):
+        ks = blocks_of(it)
+        where_from = [mod(z + offset(jnp.clip(k, 0, Z - 1)), Z) for k in ks]
+        for k, zz in zip(ks, where_from):
+            @pl.when((k >= 0) & (k < Z))
+            def _(k=k, zz=zz):
+                all_of(qbuf.at[zz, pl.ds(0, Y - 1)], qys, qyr.at[offset(k)]).wait_recv()
+
+        q = jnp.concatenate([qbuf[zz].reshape(block, 256) for zz in where_from], axis=0)
+        visible = jnp.concatenate(
+            [(key_pos <= zz * (Y * 32) + q_off) & (q_lane < 32) for zz in where_from] * 2, axis=0
+        )
+        count = 2 * block
+        stats = jnp.zeros((count, 128), jnp.float32)
         for h in range(2):
             qh = q[:, h * 128 : (h + 1) * 128]
             zero = jnp.zeros_like(qh)
@@ -276,17 +286,23 @@
             ).astype(jnp.bfloat16)
             for m in range(2):
                 combo = 2 * h + m
-                of_map = slice(m * block, (m + 1) * block)
+                of_map = slice(m * count, (m + 1) * count)
                 stats = jnp.where(lane1 == combo, top[of_map], stats)
                 stats = jnp.where(lane1 == combo + 64, tot[of_map], stats)
-                for yy in range(Y):
-                    base = m * block + yy * 16
-                    ysend[k, yy, :, combo * 128 : (combo + 1) * 128] = acc[base : base + 16]
+                for b, k in enumerate(ks):
+                    for yy in range(Y):
+                        base = m * count + b * block + yy * 16
+                        ysend[k + 1, yy, :, combo * 128 : (combo + 1) * 128] = acc[base : base + 16]
         stats = packed(stats)
-        for yy in range(Y):
-            ysend[k, yy, :, 512:] = stats[yy * 16 : yy * 16 + 16]
-        for d in range(1, Y):
-            y_copy(k, d).start()
+        for b, k in enumerate(ks):
+            for yy in range(Y):
+                base = b * block + yy * 16
+                ysend[k + 1, yy, :, 512:] = stats[base : base + 16]
+
+            @pl.when((k >= 0) & (k < Z))
+            def _(k=k):
+                for d in range(1, Y):
+                    y_copy(k, d).start()
 
     def merged(sources):
         stats = [unpacked(data[:, 512:]) for data in sources]
@@ -309,7 +325,7 @@
 
     def combine(k):
         all_of(yrecv.at[k], yds, ydr.at[k]).wait_recv()
-        top, total, outs = merged([ysend.at[k, y]] + [yrecv.at[k, i] for i in range(Y - 1)])
+        top, total, outs = merged([ysend.at[k + 1, y]] + [yrecv.at[k, i] for i in range(Y - 1)])
         for c in range(4):
             zsend[k, :, c * 128 : (c + 1) * 128] = outs[c].astype(jnp.bfloat16)
         totals = jnp.where((st_lane >= 64) & (st_lane < 68), total, 0.0)
@@ -319,19 +335,22 @@
         def _():
             z_copy(k).start()
 
-    @pl.loop(0, Z + LAG)
+    steps = Z // 2 + 1
+
+    @pl.loop(0, steps + LAG)
     def _(it):
-        @pl.when(it < Z)
+        @pl.when(it == 1)
+        def _():
+            decode()
+
+        @pl.when(it < steps)
         def _():
             chunk(it)
 
-        @pl.when(it == Z - 1)
-        def _():
-            decode()
-
-        @pl.when(it >= LAG)
-        def _():
-            combine(it - LAG)
+        for k in blocks_of(it - LAG):
+            @pl.when((k >= 0) & (k < Z))
+            def _(k=k):
+                combine(k)
 
     zall = all_of(zrecv.at[pl.ds(1, Z - 1)], zds, zdr)
     zall.wait_recv()
@@ -366,7 +385,7 @@
     all_of(qbuf.at[:, pl.ds(0, Y - 1)], qys, qyr.at[0]).wait_send()
     for copy in (p_k, p_v, p_n):
         copy.wait_send()
-    all_of(ysend.at[:, pl.ds(0, Y - 1)], yds, ydr.at[0]).wait_send()
+    all_of(ysend.at[pl.ds(1, Z), pl.ds(0, Y - 1)], yds, ydr.at[0]).wait_send()
     zall.wait_send()
     if X > 1:
         all_of(hbuf.at[pl.ds(1, X - 1)], hs, hr).wait_send()
@@ -390,7 +409,7 @@
         V((2 * slots, 128), bf), V((2 * slots, 128), bf), V((2 * npos, 128), f32),
         V((16, 512), bf), V((16, 512), bf),
         V((Z, Y, 16, 256), bf),
-        V((Z, Y, 16, 640), bf), V((Z, Y - 1, 16, 640), bf),
+        V((Z + 2, Y, 16, 640), bf), V((Z, Y - 1, 16, 640), bf),
         V((Z, 16, 640), bf), V((Z, 16, 640), bf), V((X, 32, 256), bf),
         pltpu.SMEM((2,), f32), pltpu.SMEM((1,), jnp.int32),
         S((14,)), S((3,)), S((3,)), S, S((Z,)), S, S((Z,)), S, S((Z,)), S, S, S, S,

time: 42 us -> 39.9 us (0.950)
  Pallas kernels: 37.8 us -> 35.5 us
    pallas_call x1, Pallas kernels: 37.8 us -> 35.5 us  [shards(): pl.pallas_call(functools.partial(kernel, Z, Y, X), out_shape=jax.ShapeDty...]
where the time goes in v3:
time: 39.9 us; the launch traced here: 39.4 us
  Pallas kernels  35.5 us (89%)
  local copies, waits for them, and re-layouts  2.6 us (7%)
  between operations  1.29 us (3%)
    pallas_call x1, Pallas kernels, shards(): pl.pallas_call(functools.partial(kernel, Z, Y, X), out_shape=jax.ShapeDty...  35.5 us
    slice x2, local copies, waits for them, and re-layouts, shards(): return (out[:16], out[16:17])  2.6 us

profile of v3, /device:TPU:2, one launch (start us, length us, event | category | flops | bytes accessed | tf_op | source)
XLA Modules:
  0.0 39.4 jit_solution(7464328800987959325)
XLA Ops:
  1.3 35.5 %shard_map.149 = bf16[32,512]{1,0:T(8,128)(2,1)} custom-call(bf16[16,2048]{1,0:T(8,128)(2,1)} %x_hbm.1, bf16[1,2048]{1,0:T(2,128)(2,1)} %xd_hbm.1, f32[1,2048]{1,0:T(1,128)} %bitcast.10, bf16[2048,256]{1,0:T(8,128)(2,1)} %wq_hbm.1, bf16[2048,256]{1,0:T(8,128)(2,1)} %wk_hbm.1, bf16[2048,256]{1,0:T(8,128)(2,1)} %wv_hbm.1, bf16[1024,512]{1,0:T(8,128)(2,1)} %wo_hbm.1, ...), custom_call_target="tpu_custom_call" | custom-call | tf_op jit(solution)/shard_map/pallas_call | solution.py:417
  36.8 1.3 %slice.7 = bf16[1,512]{1,0:T(2,128)(2,1)} slice(bf16[32,512]{1,0:T(8,128)(2,1)} %shard_map.149), slice={[16:17], [0:512]} | slice | bytes 2048 | tf_op jit(solution)/shard_map/slice | solution.py:429
  38.1 1.3 %slice.6 = bf16[16,512]{1,0:T(8,128)(2,1)} slice(bf16[32,512]{1,0:T(8,128)(2,1)} %shard_map.149), slice={[0:16], [0:512]} | slice | bytes 32768 | tf_op jit(solution)/shard_map/slice | solution.py:429
